TPU v7x, 512 devices: a whole 4x4x16 slice. The times are simulated.
512 devices in a mesh: sp: 32 (over z, core), tp: 16 (over y, x).
Axes of the slice: x: 4, y: 4, z: 16, core: 2. Of those that a mesh axis runs over, the one named last changes fastest.
Arguments:
- layer_input: bfloat16 [8, 4096, 2048], P(None, 'sp', 'tp'), may hold values from -6 to 6
- w_key: bfloat16 [2048, 2048], P(None, 'tp'), may hold values from -0.125 to 0.125
- w_value: bfloat16 [2048, 2048], P(None, 'tp'), may hold values from -0.125 to 0.125
- w_gates: bfloat16 [2, 2048, 16], replicated, may hold values from -0.125 to 0.125
- decay_rate: float32 [16], P('tp'), may hold values from 0 to 1, as said below
- beta_bias: float32 [16], P('tp'), may hold values from -5.5 to -3
- log_decay_extra: float32 [8, 16, 4096], P(None, 'tp', 'sp'), may hold values from -2 to 0, as said below
- new_query: bfloat16 [8, 2048], P(None, 'tp'), may hold values from -6 to 6
- read_gain: float32 [128], replicated, may hold values from 0.1 to 1.9
Outputs:
- state_cache: bfloat16 [1024, 2048], P('sp', 'tp')
- first_read: bfloat16 [8, 2048], P(None, 'tp')
Inputs may be any that keep to these rules, and one draw needn't show every extreme that they name: `decay_rate`: a positive rate for each head. `log_decay_extra`: additions that are never positive.
All inputs are finite; a program needn't handle non-finite values.
Results may differ from a plain program's by a relative error of at most 0.0052.
Values may be sent and summed in bfloat16 or wider, within the bound.
No kernel may reach another device: no remote copies, remote signals or barrier semaphores. Data moves between devices by JAX's collectives and lax.ppermute only.
A program may use at most 64 MiB of HBM per device.

v0:
```python
import jax
import jax.numpy as jnp
from jax import lax
from jax.sharding import Mesh
from jax.sharding import PartitionSpec as P

DK = 128
DV = 128
BLOCK = 64
SP = ("sp_0", "sp_1")
EPS = 1e-06
HIGH = lax.Precision.HIGHEST


def nothing_yet(x, identity):
    return jnp.broadcast_to(jnp.asarray(identity, x.dtype), x.shape)


def prefix_by_axis(x, axes, combine, identity):
    before = start = nothing_yet(x, identity)
    total = x
    for axis in reversed(axes):
        count, position = (lax.axis_size(axis), lax.axis_index(axis))
        pieces = lax.all_gather(total, axis)
        inside, total = (start, start)
        for k in reversed(range(count)):
            passed = k > position
            total = combine(total, pieces[k])
            inside = jnp.where(passed, total, inside)
        before = combine(inside, before)
    return before


def cut_along(x, dim, count):
    shape = x.shape
    pieces = x.reshape(*shape[:dim], count, shape[dim] // count, *shape[dim + 1 :])
    return jnp.moveaxis(pieces, dim, 0)


def summed_on_arrival(x, axis, dim):
    pieces = cut_along(x, dim, lax.axis_size(axis))
    arrived = lax.all_to_all(pieces, axis, split_axis=0, concat_axis=0, tiled=True)
    return arrived.sum(axis=0)


def sent_to_all(x, axis):
    count = lax.axis_size(axis)
    return lax.all_to_all(jnp.broadcast_to(x[None], (count, *x.shape)), axis, 0, 0, tiled=True)


def taken_together(x, axis):
    return sent_to_all(x, axis).sum(axis=0)


def unit_rows(values):
    return values * lax.rsqrt(jnp.sum(values * values, axis=-1, keepdims=True) + EPS)


def matmul_high(left, right):
    return jnp.einsum("...ab,...bc->...ac", left, right, precision=HIGH)


def block_pieces(keys, values, log_decay, beta):
    size = keys.shape[-2]
    width = values.shape[-1]
    running = jnp.cumsum(log_decay, axis=-1)
    sequence_indices = jnp.arange(size)
    causal = sequence_indices[:, None] >= sequence_indices[None, :]
    strict = sequence_indices[:, None] > sequence_indices[None, :]
    spread = running[..., :, None] - running[..., None, :]
    weights = jnp.where(causal, jnp.exp(jnp.where(causal, spread, 0.0)), 0.0)
    key_beta = keys * beta[..., None]
    lower = jnp.where(
        strict, jnp.einsum("...cd,...sd->...cs", key_beta, keys, precision=HIGH) * weights, 0.0
    )
    right_side = jnp.concatenate(
        [values * beta[..., None], key_beta * jnp.exp(running)[..., None]], axis=-1
    )
    solved = lax.linalg.triangular_solve(
        lower, right_side, left_side=True, lower=True, unit_diagonal=True
    )
    fresh = solved[..., :width]
    erase = solved[..., width:]
    last = running[..., -1]
    key_late = keys * jnp.exp(last[..., None] - running)[..., None]
    identity = jnp.eye(keys.shape[-1], dtype=jnp.float32)
    transition = jnp.exp(last)[..., None, None] * identity - jnp.einsum(
        "...cd,...ce->...de", key_late, erase, precision=HIGH
    )
    inject = jnp.einsum("...cd,...cv->...dv", key_late, fresh, precision=HIGH)
    return (transition, inject)


def shards(
    layer_input,
    w_key,
    w_value,
    w_gates,
    decay_rate,
    beta_bias,
    log_decay_extra,
    new_query,
    read_gain,
):
    prompts, seg_len, _ = layer_input.shape
    heads_here = w_key.shape[1] // DK
    blocks = seg_len // BLOCK
    first_head = lax.axis_index("tp") * heads_here
    gate_cols = lax.dynamic_slice_in_dim(w_gates, first_head, heads_here, 2)
    joined = jnp.concatenate([w_key, w_value], axis=1)
    piece = lax.all_gather(layer_input, "tp", axis=2, tiled=True)
    pair_sum = jnp.einsum("std,de->ste", piece, joined, preferred_element_type=jnp.float32)
    gate_sum = jnp.einsum("std,gdh->gsth", piece, gate_cols, preferred_element_type=jnp.float32)
    key_pre = pair_sum[..., : heads_here * DK].reshape(prompts, seg_len, heads_here, DK)
    value_pre = pair_sum[..., heads_here * DK :].reshape(prompts, seg_len, heads_here, DV)
    keys = unit_rows(jax.nn.silu(key_pre))
    values = jax.nn.silu(value_pre)
    log_decay = -decay_rate * jax.nn.softplus(gate_sum[0]) + log_decay_extra.transpose(0, 2, 1)
    beta = jax.nn.sigmoid(gate_sum[1] + beta_bias)
    key_blocks = keys.reshape(prompts, blocks, BLOCK, heads_here, DK).transpose(0, 3, 1, 2, 4)
    value_tiles = values.reshape(prompts, blocks, BLOCK, heads_here, DV).transpose(0, 3, 1, 2, 4)
    decay_blocks = log_decay.reshape(prompts, blocks, BLOCK, heads_here).transpose(0, 3, 1, 2)
    strength_groups = beta.reshape(prompts, blocks, BLOCK, heads_here).transpose(0, 3, 1, 2)
    transition, inject = block_pieces(key_blocks, value_tiles, decay_blocks, strength_groups)

    def compose_maps(carry, piece):
        total_map, total_add = carry
        block_map, block_add = piece
        return (
            (matmul_high(block_map, total_map), matmul_high(block_map, total_add) + block_add),
            None,
        )

    identity = jnp.eye(DK, dtype=jnp.float32)
    map_start = jnp.broadcast_to(identity, (prompts, heads_here, DK, DK))
    add_start = jnp.zeros((prompts, heads_here, DK, DV), jnp.float32)
    (seg_map, seg_add), _ = lax.scan(
        compose_maps,
        (map_start, add_start),
        (jnp.moveaxis(transition, 2, 0), jnp.moveaxis(inject, 2, 0)),
    )
    local_rows = prompts * DK // lax.axis_size(SP)
    leading_line = lax.axis_index(SP) * local_rows
    query = new_query.reshape(prompts, heads_here, DK)

    def later_first(earlier, later):
        return matmul_high(earlier, later)

    after = prefix_by_axis(seg_map, SP, later_first, map_start)
    term = jnp.einsum("shab,shbv->sahv", after, seg_add, precision=HIGH).reshape(
        prompts * DK, heads_here * DV
    )
    owned = summed_on_arrival(term, SP, 0)
    state_cache = owned.astype(jnp.bfloat16)
    query_rows = query.transpose(0, 2, 1).reshape(prompts * DK, heads_here)
    my_query = lax.dynamic_slice_in_dim(query_rows, leading_line, local_rows, 0)
    owner = (leading_line + jnp.arange(local_rows)) // DK
    member = (owner[:, None] == jnp.arange(prompts)[None, :]).astype(jnp.float32)
    weighted = my_query.astype(jnp.float32)[:, :, None] * state_cache.reshape(
        local_rows, heads_here, DV
    ).astype(jnp.float32)
    partial_read = jnp.einsum("rs,rhv->shv", member, weighted, precision=HIGH)
    raw_read = taken_together(partial_read, SP)
    scaled = (
        raw_read
        * lax.rsqrt(jnp.mean(raw_read * raw_read, axis=-1, keepdims=True) + EPS)
        * read_gain
    )
    first_read = scaled.astype(jnp.bfloat16).reshape(prompts, heads_here * DV)
    return (state_cache, first_read)


def solution(mesh):
    finer = Mesh(mesh.devices.reshape(16, 2, mesh.shape["tp"]), ("sp_0", "sp_1", "tp"))
    placed = (
        P(None, SP, "tp"),
        P(None, "tp"),
        P(None, "tp"),
        P(),
        P("tp"),
        P("tp"),
        P(None, "tp", SP),
        P(None, "tp"),
        P(),
    )
    return jax.shard_map(
        shards, mesh=finer, in_specs=placed, out_specs=(P(SP, "tp"), P(None, "tp")), check_vma=False
    )
```

profile of v0, /device:TPU:1, one launch (start us, length us, event | category | flops | bytes accessed | tf_op | source)
XLA Modules:
  0.0 407.0 jit_solution(17985307926556200827)
XLA Ops:
  7.2 0.0 copy-start
  7.2 0.0 all-gather.6.cloned.1.call-start
  7.2 0.7 all-gather.6.cloned.1.call-update
  7.9 0.0 all-gather.8.cloned.1.call-start
  9.3 0.6 broadcast.269
  9.8 1.4 reduce.14
  11.2 0.1 transpose.37
  11.4 0.1 iota_compare_fusion.4
  11.5 75.6 %all-gather.6.cloned.1.call-done = bf16[8,128,2048]{2,1,0:T(8,128)(2,1)} async-done(((bf16[8,128,128]{2,1,0:T(8,128)(2,1)}), bf16[8,128,2048]{2,1,0:T(8,128)(2,1)}) %all-gather.6.cloned.1.call-update) | async-done | bytes 4194320 | tf_op jit(solution)/shard_map/all_gather | solution.py:111
  87.1 3.4 fusion.75
  90.5 0.1 squeeze.9
  90.6 0.5 reduce_window_sum.13
  91.0 0.2 slice_reduce_fusion
  91.2 0.1 subtract_exponential_fusion
  91.3 0.1 reshape.558
  91.4 3.8 convolution_bitcast_fusion.2
  95.1 0.2 multiply_reduce_fusion
  95.4 0.3 divide_multiply_fusion
  95.7 0.1 copy.79
  95.8 1.1 fusion.13
  96.9 78.6 %custom-call.3 = f32[8,1,2,1,64,64]{4,5,3,2,1,0:T(8,128)S(1)} custom-call(f32[8,1,2,1,64,64]{5,4,3,2,1,0:T(8,128)S(1)} %fusion.13), custom_call_target="InvertDiagBlocksLowerTriangular" | custom-call | tf_op jit(solution)/shard_map/triangular_solve | solution.py:79
  175.5 0.4 broadcast_multiply_fusion
  175.9 1.1 convolution_bitcast_fusion.3
  176.9 2.0 convolution_bitcast_fusion.1
  178.9 2.0 fusion.9
  181.0 2.8 while.12
  181.1 0.6 fusion.114
  181.8 0.6 convolution_bitcast_fusion.5
  182.5 0.6 fusion.114
  183.2 0.6 convolution_bitcast_fusion.5
  183.9 0.8 copy-done.1
  184.7 0.0 all-gather.8.cloned.1.call-update
  184.7 0.2 all-gather.10.cloned.1.call-start
  184.9 21.7 %all-gather.8.cloned.1.call-done = f32[16,1,128,128]{3,2,1,0:T(8,128)} async-done(((f32[8,1,128,128]{3,2,1,0:T(8,128)}), f32[16,1,128,128]{3,2,1,0:T(8,128)}) %all-gather.8.cloned.1.call-update) | async-done | bytes 1048592 | tf_op jit(solution)/shard_map/all_gather | solution.py:24
  206.6 1.6 fusion.51
  208.3 2.5 fusion.50
  210.8 0.0 all-gather.10.cloned.1.call-update
  210.8 0.6 fusion.55
  211.5 105.1 %all-gather.10.cloned.1.call-done = f32[128,128,128]{2,1,0:T(8,128)} async-done(((f32[8,128,128]{2,1,0:T(8,128)}), f32[128,128,128]{2,1,0:T(8,128)}) %all-gather.10.cloned.1.call-update) | async-done | bytes 8388624 | tf_op jit(solution)/shard_map/all_gather | solution.py:24
  316.6 1.8 fusion.48
  318.3 2.1 fusion.46
  320.5 1.7 fusion.44
  322.2 1.7 fusion.42
  323.9 1.7 fusion.40
  325.6 1.7 fusion.38
  327.2 0.7 fusion.36
  327.9 0.7 fusion.34
  328.6 0.7 fusion.32
  329.3 0.7 fusion.30
  329.9 0.7 fusion.28
  330.6 0.7 fusion.26
  331.3 0.7 fusion.24
  332.0 0.7 fusion.22
  332.6 0.7 fusion.20
  333.3 1.3 convolution_select_fusion
  334.6 0.6 fusion.82
  335.2 1.4 fusion.52
  336.7 9.8 %all-to-all-start = ((f32[32,32,128]{2,1,0:T(8,128)}), f32[32,32,128]{2,1,0:T(8,128)S(1)}, u32[]{:S(2)}, u32[]{:S(2)}) async-start(f32[32,32,128]{2,1,0:T(8,128)} %bitcast.32), calls=%async_computation | async-start | bytes 1048576 | tf_op jit(solution)/shard_map/all_to_all | solution.py:42
  346.5 0.1 bitcast_convert_fusion
  346.6 33.4 %all-to-all-done = f32[32,32,128]{2,1,0:T(8,128)S(1)} async-done(((f32[32,32,128]{2,1,0:T(8,128)}), f32[32,32,128]{2,1,0:T(8,128)S(1)}, u32[]{:S(2)}, u32[]{:S(2)}) %all-to-all-start) | async-done | bytes 524320 | tf_op jit(solution)/shard_map/all_to_all | solution.py:42
  380.0 0.3 fusion.70
  380.3 19.3 %all_to_all.10 = f32[32,8,1,128]{3,1,2,0:T(8,128)S(1)} all-to-all(f32[32,8,1,128]{3,1,2,0:T(8,128)S(1)} %broadcast_in_dim.27), channel_id=1, replica_groups=mesh['sp_0'=16,'sp_1'=2,'tp'=16] {'sp_0','sp_1'}, dimensions={0} | all-to-all | bytes 262144 | tf_op jit(solution)/shard_map/all_to_all | solution.py:48
  399.7 0.1 multiply_reduce_fusion.1
  399.8 0.7 multiply_convert_fusion
  (34 shorter events, 0.5 us)
Async XLA Ops:
  7.2 4.2 %copy-start = (bf16[2,2048,16]{1,2,0:T(8,128)(2,1)S(1)}, bf16[2,2048,16]{1,2,0:T(8,128)(2,1)}, u32[]{:S(2)}) copy-start(bf16[2,2048,16]{1,2,0:T(8,128)(2,1)} %param.14) | copy-start | bytes 393220
  7.2 79.9 %all-gather.6.cloned.1.call-start = ((), (), s32[]{:S(2)}) async-start(), calls=%async_computation.2 | async-start | bytes 4456448 | tf_op jit(solution)/shard_map/all_gather | solution.py:111
  7.9 198.7 %all-gather.8.cloned.1.call-start = ((), (), s32[]{:S(2)}) async-start(), calls=%async_computation.3 | async-start | bytes 1572864 | tf_op jit(solution)/shard_map/all_gather | solution.py:24
  183.9 0.8 copy-start.1
  184.7 131.9 %all-gather.10.cloned.1.call-start = ((), (), s32[]{:S(2)}) async-start(), calls=%async_computation.4 | async-start | bytes 8912896 | tf_op jit(solution)/shard_map/all_gather | solution.py:24
  316.6 10.7 %copy-start.2 = (f32[128,128,128]{2,1,0:T(8,128)S(1)}, f32[128,128,128]{2,1,0:T(8,128)}, u32[]{:S(2)}) copy-start(f32[128,128,128]{2,1,0:T(8,128)} %all-gather.10.cloned.1.call-done) | copy-start | bytes 25165828
  331.9 14.5 %copy-start.4 = (bf16[8,128]{1,0:T(8,128)(2,1)S(1)}, bf16[8,128]{1,0:T(8,128)(2,1)}, u32[]{:S(2)}) copy-start(bf16[8,128]{1,0:T(8,128)(2,1)} %param.18) | copy-start | bytes 6148
  331.9 67.8 %copy-start.5 = (f32[128]{0:T(128)S(1)}, f32[128]{0:T(128)}, u32[]{:S(2)}) copy-start(f32[128]{0:T(128)} %param.19) | copy-start | bytes 1540
  336.7 43.3 %all-to-all-start = ((f32[32,32,128]{2,1,0:T(8,128)}), f32[32,32,128]{2,1,0:T(8,128)S(1)}, u32[]{:S(2)}, u32[]{:S(2)}) async-start(f32[32,32,128]{2,1,0:T(8,128)} %bitcast.32), calls=%async_computation | async-start | bytes 1048576 | tf_op jit(solution)/shard_map/all_to_all | solution.py:42
  380.0 20.4 %copy-start.3 = (bf16[32,128]{1,0:T(8,128)(2,1)}, bf16[32,128]{1,0:T(8,128)(2,1)S(1)}, u32[]{:S(2)}) copy-start(bf16[32,128]{1,0:T(8,128)(2,1)S(1)} %reduce_sum.37) | copy-start | bytes 24580
Sparse Core Ops, SparseCore 0:
  11.0 76.0 all-gather.5
  184.8 21.7 all-gather.7
  210.9 105.5 all-gather.9
where the time goes:
time: 408 us; the launch traced here: 407 us
  waiting for transfers between devices  236 us (58%)
  other arithmetic  82.5 us (20%)
  matrix products  40.8 us (10%)
  blocking collectives  19.3 us (5%)
  between operations  15.5 us (4%)
  starting transfers between devices  10.1 us (2%)
    all_gather x2, waiting for transfers between devices, prefix_by_axis(): pieces = lax.all_gather(total, axis)  127 us
    another operation x3, other arithmetic, block_pieces(): lax.linalg.triangular_solve(lower, right_side, left_side=True, lower=True...  78.7 us
    all_gather x1, waiting for transfers between devices, shards(): piece = lax.all_gather(layer_input, 'tp', axis=2, tiled=True)  75.6 us
    all_to_all x1, waiting for transfers between devices, summed_on_arrival(): lax.all_to_all(pieces, axis, split_axis=0, concat_axis=0, tiled=True)  33.4 us
    dot_general x24, matrix products, matmul_high(): return jnp.einsum('...ab,...bc->...ac', left, right, precision=HIGH)  25.9 us
    all_to_all x1, blocking collectives, sent_to_all(): lax.all_to_all(jnp.broadcast_to(x[None], (count, *x.shape)), axis, 0, 0,...  19.3 us
    all_to_all x1, starting transfers between devices, summed_on_arrival(): lax.all_to_all(pieces, axis, split_axis=0, concat_axis=0, tiled=True)  9.76 us
  transfers between devices with their start and end apart: 4, of which 4 were waited for; matrix products, arithmetic and copies ran while one was open for 1% of the time, Pallas kernels for 0%

commit v1 on v0

--- a/solution.py
+++ b/solution.py
@@ -108,7 +108,9 @@
     first_head = lax.axis_index("tp") * heads_here
     gate_cols = lax.dynamic_slice_in_dim(w_gates, first_head, heads_here, 2)
     joined = jnp.concatenate([w_key, w_value], axis=1)
-    piece = lax.all_gather(layer_input, "tp", axis=2, tiled=True)
+    piece = jnp.concatenate(
+        lax.all_to_all(jnp.stack([layer_input] * lax.axis_size("tp")), "tp", 0, 0), axis=2
+    )
     pair_sum = jnp.einsum("std,de->ste", piece, joined, preferred_element_type=jnp.float32)
     gate_sum = jnp.einsum("std,gdh->gsth", piece, gate_cols, preferred_element_type=jnp.float32)
     key_pre = pair_sum[..., : heads_here * DK].reshape(prompts, seg_len, heads_here, DK)

time: 408 us -> 404 us (level)
  waiting for transfers between devices: 236 us -> 222 us
  starting transfers between devices: 10.1 us -> 17.6 us
    all_gather x1 -> x0, waiting for transfers between devices: 75.6 us -> none  [shards(): piece = lax.all_gather(layer_input, 'tp', axis=2, tiled=True)]
    all_to_all x0 -> x1, waiting for transfers between devices: none -> 51.2 us  [shards(): lax.all_to_all(jnp.stack([layer_input] * lax.axis_size('tp')), 'tp', 0, 0)]
    all_gather x2, waiting for transfers between devices: 127 us -> 138 us  [prefix_by_axis(): pieces = lax.all_gather(total, axis)]
    all_to_all x0 -> x1, starting transfers between devices: none -> 7.62 us  [shards(): lax.all_to_all(jnp.stack([layer_input] * lax.axis_size('tp')), 'tp', 0, 0)]
  transfers between devices with their start and end apart: 4 -> 4, of which waited for: 4 -> 4; matrix products, arithmetic and copies ran while one was open for 1% -> 0% of each run, Pallas kernels for 0% -> 0%
where the time goes in v1:
time: 404 us
  waiting for transfers between devices  222 us (55%)
  other arithmetic  81.7 us (20%)
  matrix products  40.5 us (10%)
  blocking collectives  19.3 us (5%)
  starting transfers between devices  17.6 us (4%)
  between operations  15.8 us (4%)
  local copies, waits for them, and re-layouts  6.18 us (2%)
    all_gather x2, waiting for transfers between devices, prefix_by_axis(): pieces = lax.all_gather(total, axis)  138 us
    another operation x3, other arithmetic, block_pieces(): lax.linalg.triangular_solve(lower, right_side, left_side=True, lower=True...  78.7 us
    all_to_all x1, waiting for transfers between devices, shards(): lax.all_to_all(jnp.stack([layer_input] * lax.axis_size('tp')), 'tp', 0, 0)  51.2 us
    all_to_all x1, waiting for transfers between devices, summed_on_arrival(): lax.all_to_all(pieces, axis, split_axis=0, concat_axis=0, tiled=True)  33.4 us
    dot_general x24, matrix products, matmul_high(): return jnp.einsum('...ab,...bc->...ac', left, right, precision=HIGH)  25.9 us
    all_to_all x1, blocking collectives, sent_to_all(): lax.all_to_all(jnp.broadcast_to(x[None], (count, *x.shape)), axis, 0, 0,...  19.3 us
    all_to_all x1, starting transfers between devices, summed_on_arrival(): lax.all_to_all(pieces, axis, split_axis=0, concat_axis=0, tiled=True)  9.76 us
  transfers between devices with their start and end apart: 4, of which 4 were waited for; matrix products, arithmetic and copies ran while one was open for 0% of the time, Pallas kernels for 0%

profile of v1, /device:TPU:1, one launch (start us, length us, event | category | flops | bytes accessed | tf_op | source)
XLA Modules:
  0.0 403.7 jit_solution(4428323477088397952)
XLA Ops:
  7.2 0.0 copy-start
  7.2 4.1 %stack.2 = bf16[16,8,128,128]{3,2,1,0:T(8,128)(2,1)} broadcast(bf16[8,128,128]{2,1,0:T(8,128)(2,1)} %param.11), dimensions={1,2,3} | broadcast | bytes 4456448 | tf_op jit(solution)/shard_map/stack | solution.py:112
  11.3 7.6 %all-to-all-start = ((bf16[16,8,128,128]{3,2,1,0:T(8,128)(2,1)}), bf16[16,8,128,128]{3,2,1,0:T(8,128)(2,1)}, u32[]{:S(2)}, u32[]{:S(2)}) async-start(bf16[16,8,128,128]{3,2,1,0:T(8,128)(2,1)} %stack.2), calls=%async_computation | async-start | bytes 8388608 | tf_op jit(solution)/shard_map/all_to_all | solution.py:112
  18.9 0.0 all-gather.5.cloned.1.call-start
  20.3 0.5 broadcast.271
  20.7 0.6 reduce.14
  21.3 0.1 transpose.37
  21.5 0.1 iota_compare_fusion.4
  21.6 51.2 %all-to-all-done = bf16[16,8,128,128]{3,2,1,0:T(8,128)(2,1)} async-done(((bf16[16,8,128,128]{3,2,1,0:T(8,128)(2,1)}), bf16[16,8,128,128]{3,2,1,0:T(8,128)(2,1)}, u32[]{:S(2)}, u32[]{:S(2)}) %all-to-all-start) | async-done | bytes 4194336 | tf_op jit(solution)/shard_map/all_to_all | solution.py:112
  72.8 3.4 fusion.11
  76.2 0.1 squeeze.9
  76.3 0.5 reduce_window_sum.13
  76.7 0.2 slice_reduce_fusion
  76.9 0.1 subtract_exponential_fusion
  77.0 0.1 reshape.568
  77.1 3.4 fusion.15
  80.5 0.2 multiply_reduce_fusion
  80.8 0.3 divide_multiply_fusion
  81.1 0.1 copy.82
  81.2 1.1 fusion.22
  82.2 78.6 %custom-call.3 = f32[8,1,2,1,64,64]{4,5,3,2,1,0:T(8,128)S(1)} custom-call(f32[8,1,2,1,64,64]{5,4,3,2,1,0:T(8,128)S(1)} %fusion.22), custom_call_target="InvertDiagBlocksLowerTriangular" | custom-call | tf_op jit(solution)/shard_map/triangular_solve | solution.py:79
  160.9 0.4 broadcast_multiply_fusion
  161.3 1.1 convolution_bitcast_fusion.2
  162.4 2.0 convolution_bitcast_fusion.1
  164.4 2.0 fusion.18
  166.5 2.8 while.12
  166.6 0.6 fusion.122
  167.2 0.6 convolution_bitcast_fusion.4
  168.0 0.6 fusion.122
  168.6 0.6 convolution_bitcast_fusion.4
  169.3 0.8 copy-done.1
  170.1 0.0 all-gather.5.cloned.1.call-update
  170.1 0.2 all-gather.7.cloned.1.call-start
  170.4 32.7 %all-gather.5.cloned.1.call-done = f32[16,1,128,128]{3,2,1,0:T(8,128)} async-done(((f32[8,1,128,128]{3,2,1,0:T(8,128)}), f32[16,1,128,128]{3,2,1,0:T(8,128)}) %all-gather.5.cloned.1.call-update) | async-done | bytes 1048592 | tf_op jit(solution)/shard_map/all_gather | solution.py:24
  203.0 1.6 fusion.60
  204.7 2.5 fusion.59
  207.2 0.0 all-gather.7.cloned.1.call-update
  207.3 0.6 fusion.64
  207.9 105.1 %all-gather.7.cloned.1.call-done = f32[128,128,128]{2,1,0:T(8,128)} async-done(((f32[8,128,128]{2,1,0:T(8,128)}), f32[128,128,128]{2,1,0:T(8,128)}) %all-gather.7.cloned.1.call-update) | async-done | bytes 8388624 | tf_op jit(solution)/shard_map/all_gather | solution.py:24
  313.0 1.8 fusion.57
  314.8 2.1 fusion.55
  316.9 1.7 fusion.53
  318.6 1.7 fusion.51
  320.3 1.7 fusion.49
  322.0 1.7 fusion.47
  323.7 0.7 fusion.45
  324.3 0.7 fusion.43
  325.0 0.7 fusion.41
  325.7 0.7 fusion.39
  326.4 0.7 fusion.37
  327.0 0.7 fusion.35
  327.7 0.7 fusion.33
  328.4 0.7 fusion.31
  329.1 0.7 fusion.29
  329.7 1.3 convolution_select_fusion
  331.0 0.7 fusion.90
  331.7 1.4 fusion.61
  333.1 9.8 %all-to-all-start.1 = ((f32[32,32,128]{2,1,0:T(8,128)}), f32[32,32,128]{2,1,0:T(8,128)S(1)}, u32[]{:S(2)}, u32[]{:S(2)}) async-start(f32[32,32,128]{2,1,0:T(8,128)} %bitcast.33), calls=%async_computation.1 | async-start | bytes 1048576 | tf_op jit(solution)/shard_map/all_to_all | solution.py:42
  342.9 0.1 bitcast_convert_fusion
  343.0 33.4 %all-to-all-done.1 = f32[32,32,128]{2,1,0:T(8,128)S(1)} async-done(((f32[32,32,128]{2,1,0:T(8,128)}), f32[32,32,128]{2,1,0:T(8,128)S(1)}, u32[]{:S(2)}, u32[]{:S(2)}) %all-to-all-start.1) | async-done | bytes 524320 | tf_op jit(solution)/shard_map/all_to_all | solution.py:42
  376.4 0.3 fusion.79
  376.7 19.3 %all_to_all.15 = f32[32,8,1,128]{3,1,2,0:T(8,128)S(1)} all-to-all(f32[32,8,1,128]{3,1,2,0:T(8,128)S(1)} %broadcast_in_dim.27), channel_id=1, replica_groups=mesh['sp_0'=16,'sp_1'=2,'tp'=16] {'sp_0','sp_1'}, dimensions={0} | all-to-all | bytes 262144 | tf_op jit(solution)/shard_map/all_to_all | solution.py:48
  396.1 0.1 multiply_reduce_fusion.1
  396.2 0.7 multiply_convert_fusion
  (40 shorter events, 0.5 us)
Async XLA Ops:
  7.2 14.3 %copy-start = (bf16[2,2048,16]{1,2,0:T(8,128)(2,1)S(1)}, bf16[2,2048,16]{1,2,0:T(8,128)(2,1)}, u32[]{:S(2)}) copy-start(bf16[2,2048,16]{1,2,0:T(8,128)(2,1)} %param.14) | copy-start | bytes 393220
  7.2 13.6 %copy-start.4 = (f32[8,1,128]{2,1,0:T(1,128)S(1)}, f32[8,1,128]{2,1,0:T(1,128)}, u32[]{:S(2)}) copy-start(f32[8,1,128]{2,1,0:T(1,128)} %param.17) | copy-start | bytes 12292
  7.2 69.9 %copy-start.7 = (bf16[2048,128]{1,0:T(8,128)(2,1)S(1)}, bf16[2048,128]{1,0:T(8,128)(2,1)}, u32[]{:S(2)}) copy-start(bf16[2048,128]{1,0:T(8,128)(2,1)} %param.13) | copy-start | bytes 1572868
  7.2 69.9 %copy-start.8 = (bf16[2048,128]{1,0:T(8,128)(2,1)S(1)}, bf16[2048,128]{1,0:T(8,128)(2,1)}, u32[]{:S(2)}) copy-start(bf16[2048,128]{1,0:T(8,128)(2,1)} %param.12) | copy-start | bytes 1572868
  11.3 61.5 %all-to-all-start = ((bf16[16,8,128,128]{3,2,1,0:T(8,128)(2,1)}), bf16[16,8,128,128]{3,2,1,0:T(8,128)(2,1)}, u32[]{:S(2)}, u32[]{:S(2)}) async-start(bf16[16,8,128,128]{3,2,1,0:T(8,128)(2,1)} %stack.2), calls=%async_computation | async-start | bytes 8388608 | tf_op jit(solution)/shard_map/all_to_all | solution.py:112
  18.9 184.1 %all-gather.5.cloned.1.call-start = ((), (), s32[]{:S(2)}) async-start(), calls=%async_computation.3 | async-start | bytes 1572864 | tf_op jit(solution)/shard_map/all_gather | solution.py:24
  169.3 0.8 copy-start.1
  170.1 142.9 %all-gather.7.cloned.1.call-start = ((), (), s32[]{:S(2)}) async-start(), calls=%async_computation.4 | async-start | bytes 8912896 | tf_op jit(solution)/shard_map/all_gather | solution.py:24
  313.0 10.7 %copy-start.2 = (f32[128,128,128]{2,1,0:T(8,128)S(1)}, f32[128,128,128]{2,1,0:T(8,128)}, u32[]{:S(2)}) copy-start(f32[128,128,128]{2,1,0:T(8,128)} %all-gather.7.cloned.1.call-done) | copy-start | bytes 25165828
  328.4 14.5 %copy-start.5 = (bf16[8,128]{1,0:T(8,128)(2,1)S(1)}, bf16[8,128]{1,0:T(8,128)(2,1)}, u32[]{:S(2)}) copy-start(bf16[8,128]{1,0:T(8,128)(2,1)} %param.18) | copy-start | bytes 6148
  328.4 67.8 %copy-start.6 = (f32[128]{0:T(128)S(1)}, f32[128]{0:T(128)}, u32[]{:S(2)}) copy-start(f32[128]{0:T(128)} %param.19) | copy-start | bytes 1540
  333.1 43.3 %all-to-all-start.1 = ((f32[32,32,128]{2,1,0:T(8,128)}), f32[32,32,128]{2,1,0:T(8,128)S(1)}, u32[]{:S(2)}, u32[]{:S(2)}) async-start(f32[32,32,128]{2,1,0:T(8,128)} %bitcast.33), calls=%async_computation.1 | async-start | bytes 1048576 | tf_op jit(solution)/shard_map/all_to_all | solution.py:42
  376.4 20.4 %copy-start.3 = (bf16[32,128]{1,0:T(8,128)(2,1)}, bf16[32,128]{1,0:T(8,128)(2,1)S(1)}, u32[]{:S(2)}) copy-start(bf16[32,128]{1,0:T(8,128)(2,1)S(1)} %reduce_sum.37) | copy-start | bytes 24580
Sparse Core Ops, SparseCore 0:
  170.2 32.7 all-gather.4
  207.3 105.5 all-gather.6
